TPU v7x, 32 devices: a whole 2x2x4 slice. The times are simulated.
32 devices in a mesh: grp: 2 (over y), st: 4 (over z), tp: 4 (over x, core).
Axes of the slice: x: 2, y: 2, z: 4, core: 2. Of those that a mesh axis runs over, the one named last changes fastest.
Arguments:
- tokens: bfloat16 [8192, 2048], P(('grp', 'st'), 'tp'), parts along dimension 0, may hold values from -6 to 6
- norm_gain: float32 [2048], replicated, may hold values from 0.1 to 1.9
- pool_weight: bfloat16 [4, 512, 512], P('tp'), may hold values from -0.25 to 0.25
- pool_scale: float32 [2048], P('tp'), may hold values from 0.1 to 1.9
- query_weight: bfloat16 [2048, 1024], P(None, 'tp'), may hold values from -3 to 3
- gate_weight: bfloat16 [2048, 8], replicated, may hold values from -0.125 to 0.125
- key_weight: bfloat16 [2048, 1024], P(None, 'tp'), may hold values from -0.125 to 0.125
- value_weight: bfloat16 [2048, 1024], P(None, 'tp'), may hold values from -0.125 to 0.125
- out_weight: bfloat16 [1024, 2048], P(None, 'tp'), may hold values from -0.1875 to 0.1875
- passage_gain: float32 [2048], replicated, may hold values from 0.1 to 1.9
- passage_store: bfloat16 [192, 64, 2048], P(('grp', 'st')), parts along dimension 0, may hold values from -6 to 6
- passage_ids: int32 [64, 4], P(('grp', 'st')), parts along dimension 0, may hold values from 0 to 95, as said below
Outputs:
- mixed: bfloat16 [8192, 2048], P(('grp', 'st'), 'tp'), parts along dimension 0
There are 2 independent parts, one for each index of `grp`. A program takes and returns all parts, laid end to end along the dimension named above; an argument that names none is the same for every part. Nothing has to cross between parts.
Inputs may be any that keep to these rules, and one draw needn't show every extreme that they name: `passage_ids`: the ids of the blocks of one index of st name at most 8 passages held by any one index of st, and exactly 8 held by some index.
All inputs are finite; a program needn't handle non-finite values.
Results may differ from a plain program's by a relative error of at most 0.009.
Values may be sent and summed in bfloat16 or wider, within the bound.
A program may use at most 128 MiB of HBM per device.

v0:
```python
import jax
import jax.numpy as jnp
from jax import lax
from jax.sharding import PartitionSpec as P

HD = 128
GROUPS = 4
SEQ_LEN = 256
BLK = 128
NPB = 4
PLEN = 64
P_DEV = 24


epsilon = 1e-06


def normalize_rows(fetched, passage_gain):
    wide_rows = fetched.astype(jnp.float32)
    inverse = lax.rsqrt(jnp.mean(wide_rows * wide_rows, axis=-1, keepdims=True) + epsilon)
    return (wide_rows * inverse * passage_gain).astype(jnp.bfloat16)


def project_rows(fetched, passage_gain, both_weights):
    count_rows = fetched.shape[0]
    flat_rows = normalize_rows(fetched.reshape(count_rows * PLEN, fetched.shape[2]), passage_gain)
    projected = jnp.dot(flat_rows, both_weights, preferred_element_type=jnp.float32).astype(
        jnp.bfloat16
    )
    return projected.reshape(count_rows, PLEN, both_weights.shape[1])


def per_device(
    tokens,
    norm_gain,
    pool_weight,
    pool_scale,
    query_weight,
    gate_weight,
    key_weight,
    value_weight,
    out_weight,
    passage_gain,
    passage_store,
    passage_ids,
):
    head_index = lax.axis_index("tp")
    tok_rows, width_local = tokens.shape
    full_width = width_local * lax.axis_size("tp")
    local_heads = query_weight.shape[1] // HD
    head_width = local_heads * HD
    wide_tokens = tokens.astype(jnp.float32)
    square_sums = lax.psum(jnp.sum(wide_tokens * wide_tokens, axis=1), "tp")
    inverse = lax.rsqrt(square_sums / full_width + epsilon)
    gain_local = lax.dynamic_slice_in_dim(norm_gain, head_index * width_local, width_local)
    normed = (wide_tokens * inverse[:, None] * gain_local[None, :]).astype(jnp.bfloat16)
    sequences = tok_rows // SEQ_LEN
    widest = 2**GROUPS
    window = jnp.left_shift(jnp.int32(2), head_index)
    grouped = normed.astype(jnp.float32).reshape(sequences, SEQ_LEN, width_local)
    running = jnp.cumsum(grouped, axis=1)
    padded = jnp.concatenate(
        [jnp.zeros((sequences, widest, width_local), jnp.float32), running], axis=1
    )
    lagged = lax.dynamic_slice_in_dim(padded, widest - window, SEQ_LEN, axis=1)
    position = jnp.arange(SEQ_LEN, dtype=jnp.int32)
    divisor = jnp.minimum(position + 1, window).astype(jnp.float32)
    pooled = (
        ((running - lagged) / divisor[None, :, None] - grouped)
        .astype(jnp.bfloat16)
        .reshape(tok_rows, width_local)
    )
    mixing = (
        jnp.dot(pooled, pool_weight[0], preferred_element_type=jnp.float32) * pool_scale[None, :]
    )
    gate_columns = lax.dynamic_slice_in_dim(
        gate_weight, head_index * local_heads, local_heads, axis=1
    )
    columns = lax.all_gather(normed, "tp", axis=1, tiled=True)
    query_sum = jnp.dot(columns, query_weight, preferred_element_type=jnp.float32)
    gate_sum = jnp.dot(columns, gate_columns, preferred_element_type=jnp.float32)
    queries = query_sum.astype(jnp.bfloat16)
    gating = jax.nn.sigmoid(gate_sum)
    flat_ids = passage_ids.reshape(-1)
    asked_count = flat_ids.shape[0]
    st_count = lax.axis_size("st")
    capacity = max(2, (asked_count + st_count - 1) // st_count)
    owners = flat_ids // P_DEV
    local_index = flat_ids % P_DEV
    order_index = jnp.arange(asked_count, dtype=jnp.int32)
    earlier = (owners[None, :] == owners[:, None]) & (order_index[None, :] < order_index[:, None])
    slot_index = jnp.sum(earlier.astype(jnp.int32), axis=1)
    position_flat = owners * capacity + slot_index
    slot_range = jnp.arange(st_count * capacity, dtype=jnp.int32)
    request_table = jnp.sum(
        jnp.where(position_flat[None, :] == slot_range[:, None], local_index[None, :], 0), axis=1
    )
    request_table = request_table.reshape(st_count, capacity)
    asked = lax.all_to_all(request_table, "st", split_axis=0, concat_axis=0, tiled=True)
    both_weights = jnp.concatenate([key_weight, value_weight], axis=1)
    projected_store = project_rows(passage_store, passage_gain, both_weights)
    projected = jnp.take(projected_store, asked.reshape(-1), axis=0)
    returned = lax.all_to_all(
        projected.reshape(st_count, capacity * PLEN, 2 * head_width),
        "st",
        split_axis=0,
        concat_axis=0,
        tiled=True,
    )
    key_values = jnp.take(
        returned.reshape(st_count * capacity, PLEN, 2 * head_width), position_flat, axis=0
    )
    block_count = tok_rows // BLK
    key_values = key_values.reshape(block_count, NPB * PLEN, 2 * head_width)
    key_rows = key_values[:, :, :head_width].reshape(block_count, NPB * PLEN, local_heads, HD)
    values = key_values[:, :, head_width:].reshape(block_count, NPB * PLEN, local_heads, HD)
    query_blocks = queries.reshape(block_count, BLK, local_heads, HD)
    scores = jnp.einsum(
        "bqhd,bkhd->bhqk", query_blocks, key_rows, preferred_element_type=jnp.float32
    ) * HD ** (-0.5)
    row_max = jnp.max(scores, axis=-1, keepdims=True)
    weights = jnp.exp(scores - row_max)
    probabilities = (weights / jnp.sum(weights, axis=-1, keepdims=True)).astype(jnp.bfloat16)
    attended = jnp.einsum(
        "bhqk,bkhd->bqhd", probabilities, values, preferred_element_type=jnp.float32
    ).reshape(tok_rows, local_heads, HD)
    head_out = (attended * gating[:, :, None]).astype(jnp.bfloat16).reshape(tok_rows, head_width)
    crossed = jnp.dot(
        lax.all_gather(head_out, "tp", axis=1, tiled=True),
        out_weight,
        preferred_element_type=jnp.float32,
    )
    return (mixing + crossed).astype(jnp.bfloat16)


def solution(mesh):
    in_specs = (
        P(("grp", "st"), "tp"),
        P(),
        P("tp", None, None),
        P("tp"),
        P(None, "tp"),
        P(),
        P(None, "tp"),
        P(None, "tp"),
        P(None, "tp"),
        P(),
        P(("grp", "st"), None, None),
        P(("grp", "st"), None),
    )
    out_specs = P(("grp", "st"), "tp")
    return jax.shard_map(
        per_device, mesh=mesh, in_specs=in_specs, out_specs=out_specs, check_vma=False
    )
```

profile of v0, /device:TPU:0, one launch (start us, length us, event | category | flops | bytes accessed | tf_op | source)
XLA Modules:
  0.0 155.8 jit_solution(16865734827480352059)
XLA Ops:
  6.5 0.0 copy-start
  6.5 0.8 copy.41
  7.4 0.1 ne.86
  7.5 0.1 rem.47
  7.6 0.1 div.68
  7.7 0.2 convert_reduce_fusion
  7.9 0.1 select_reduce_fusion
  8.0 0.7 all_to_all.9
  8.6 6.3 %all-to-all-start = ((s32[4,1,8]{2,1,0:T(1,128)}), s32[4,1,8]{2,1,0:T(1,128)S(1)}, u32[]{:S(2)}, u32[]{:S(2)}) async-start(s32[4,1,8]{2,1,0:T(1,128)} %bitcast.9), calls=%async_computation | async-start | bytes 4096 | tf_op jit(solution)/shard_map/all_to_all | solution.py:99
  15.0 0.0 all-gather.3.cloned.1.call-start
  15.0 1.5 fusion.6
  16.5 6.5 %psum.7 = f32[1024]{0:T(1024)S(1)} all-reduce(f32[1024]{0:T(1024)S(1)} %fusion.6), channel_id=1, replica_groups=mesh['grp'=2,'st'=4,'tp'=4] {'tp'}, use_global_device_ids=true, to_apply=%region_1.0 | all-reduce | flops 1024 | bytes 8192 | tf_op jit(solution)/shard_map/psum | solution.py:53
  23.0 0.8 dynamic_slice.9
  23.8 2.5 %fusion.8 = bf16[1024,512]{1,0:T(8,128)(2,1)} fusion(bf16[1024,512]{1,0:T(8,128)(2,1)} %param.12, f32[512]{0:T(512)S(1)} %dynamic_slice.9, f32[1024]{0:T(1024)S(1)} %add_rsqrt_fusion.1), kind=kLoop, calls=%fused_computation.16 | loop fusion | flops 2097152 | bytes 2103296 | tf_op jit(solution)/shard_map/convert_element_type | solution.py:56
  26.3 0.0 all-gather.3.cloned.1.call-update
  26.3 0.0 copy-start.4
  26.4 4.1 %multiply_reduce_fusion = f32[24,64]{1,0:T(8,128)S(1)} fusion(bf16[24,64,2048]{2,1,0:T(8,128)(2,1)} %param.22), kind=kLoop, calls=%fused_computation.6 | loop fusion | flops 9435648 | bytes 6297600 | tf_op jit(solution)/shard_map/reduce_sum | solution.py:20
  30.4 0.1 rsqrt.16
  30.5 4.6 %fusion.2 = bf16[1536,2048]{1,0:T(8,128)(2,1)S(1)} fusion(f32[2048]{0:T(1024)S(1)} %copy-done.4, f32[1536]{0:T(1024)S(1)} %rsqrt.16, bf16[24,64,2048]{2,1,0:T(8,128)(2,1)} %param.22), kind=kLoop, calls=%fused_computation.5 | loop fusion | flops 12582912 | bytes 12597248 | tf_op jit(solution)/shard_map/convert_element_type | solution.py:21
  35.1 4.8 %convolution_convert_fusion = bf16[1536,512]{1,0:T(8,128)(2,1)} fusion(bf16[1536,2048]{1,0:T(8,128)(2,1)S(1)} %fusion.2, bf16[2048,256]{1,0:T(8,128)(2,1)S(1)} %copy-done.6, bf16[2048,256]{1,0:T(8,128)(2,1)S(1)} %copy-done.7), kind=kOutput, calls=%fused_computation.7 | convolution fusion | flops 3226206208 | bytes 9961472 | tf_op jit(solution)/shard_map/dot_general | solution.py:27
  39.9 0.0 all-to-all-done
  39.9 0.5 broadcast.275
  40.4 0.7 reduce.4
  41.1 0.1 reshape.267
  41.2 0.1 broadcast_in_dim.62
  41.3 0.1 broadcast_in_dim.63
  41.4 2.1 %gather_fusion = bf16[32,64,512]{2,1,0:T(8,128)(2,1)S(1)} fusion(bf16[24,64,512]{2,1,0:T(8,128)(2,1)} %bitcast.73, s32[1024]{0:T(1024)S(1)} %pad_clamp_fusion.1), kind=kCustom, calls=%fused_computation | custom fusion | bytes 4194432 | tf_op jit(solution)/shard_map/jit(_take)/gather | solution.py:102
  43.5 1.6 %bitcast_select_fusion.1 = bf16[4,512,512]{2,1,0:T(8,128)(2,1)} fusion(pred[4,512]{1,0:T(4,128)(4,1)S(1)} %broadcast_in_dim.63, bf16[4,512,512]{2,1,0:T(8,128)(2,1)S(1)} %bitcast.66), kind=kLoop, calls=%fused_computation.21 | loop fusion | flops 1048576 | bytes 4196352 | tf_op jit(solution)/shard_map/jit(_take)/select_n | solution.py:102
  45.1 4.5 %all-to-all-start.1 = ((bf16[4,512,512]{2,1,0:T(8,128)(2,1)}), bf16[4,512,512]{2,1,0:T(8,128)(2,1)S(1)}, u32[]{:S(2)}, u32[]{:S(2)}) async-start(bf16[4,512,512]{2,1,0:T(8,128)(2,1)} %bitcast_select_fusion.1), calls=%async_computation.1 | async-start | bytes 4194304 | tf_op jit(solution)/shard_map/all_to_all | solution.py:103
  49.6 0.1 div.71
  49.7 0.1 reduce_sum.51
  49.8 0.1 and.63
  49.9 0.1 broadcast_in_dim.57
  49.9 0.1 broadcast_in_dim.58
  50.1 47.4 %all-to-all-done.1 = bf16[4,512,512]{2,1,0:T(8,128)(2,1)S(1)} async-done(((bf16[4,512,512]{2,1,0:T(8,128)(2,1)}), bf16[4,512,512]{2,1,0:T(8,128)(2,1)S(1)}, u32[]{:S(2)}, u32[]{:S(2)}) %all-to-all-start.1) | async-done | bytes 2097184 | tf_op jit(solution)/shard_map/all_to_all | solution.py:103
  97.4 2.0 %gather_fusion.1 = bf16[32,64,512]{2,1,0:T(8,128)(2,1)} fusion(bf16[32,64,512]{2,1,0:T(8,128)(2,1)S(1)} %bitcast.65, s32[1024]{0:T(1024)S(1)} %pad_clamp_fusion), kind=kCustom, calls=%fused_computation.1 | custom fusion | bytes 4194432 | tf_op jit(solution)/shard_map/jit(_take)/gather | solution.py:110
  99.4 1.8 %bitcast_select_fusion = bf16[8,256,512]{2,1,0:T(8,128)(2,1)S(1)} fusion(pred[8,256]{1,0:T(8,128)(4,1)S(1)} %broadcast_in_dim.58, bf16[8,256,512]{2,1,0:T(8,128)(2,1)} %bitcast.67), kind=kLoop, calls=%fused_computation.20 | loop fusion | flops 1048576 | bytes 4196352 | tf_op jit(solution)/shard_map/jit(_take)/select_n | solution.py:110
  101.2 1.2 fusion.46
  102.4 1.5 copy.46
  103.9 1.3 copy.45
  105.2 3.7 %convolution_convert_fusion.1 = bf16[1024,256]{1,0:T(8,128)(2,1)S(1)} fusion(bf16[1024,2048]{1,0:T(8,128)(2,1)} %all-gather.3.cloned.1.call-done, bf16[2048,256]{1,0:T(8,128)(2,1)} %param.16), kind=kOutput, calls=%fused_computation.31 | convolution fusion | flops 1074003968 | bytes 5767168 | tf_op jit(solution)/shard_map/dot_general | solution.py:80
  108.9 0.1 reshape.270
  109.1 1.0 fusion.47
  110.1 1.8 %fusion.22 = f32[8,2,128,256]{3,2,1,0:T(8,128)} fusion(bf16[8,256,2,128]{1,3,2,0:T(8,128)(2,1)S(1)} %bitcast.70, bf16[8,128,2,128]{3,2,1,0:T(2,128)(2,1)S(1)} %reshape.270), kind=kOutput, calls=%fused_computation.41 | convolution fusion | flops 134217728 | bytes 3670016 | tf_op jit(solution)/shard_map/bqhd,bkhd->bhqk/dot_general | solution.py:118
  111.8 5.7 %convolution_bitcast_fusion = f32[8,128,2,128]{1,3,2,0:T(8,128)S(1)} fusion(bf16[8,256,2,128]{1,3,2,0:T(8,128)(2,1)} %bitcast.74, f32[8,2,128]{2,1,0:T(2,128)S(1)} %fusion.47, f32[8,2,128,256]{3,2,1,0:T(8,128)} %fusion.22), kind=kOutput, calls=%fused_computation.30 | convolution fusion | flops 136317184 | bytes 4202496 | tf_op jit(solution)/shard_map/bhqk,bkhd->bqhd/dot_general | solution.py:124
  117.5 0.6 copy.49
  118.1 3.4 %fusion.18 = f32[1024,2]{0,1:T(2,128)S(1)} fusion(bf16[1024,2048]{1,0:T(8,128)(2,1)} %all-gather.3.cloned.1.call-done, bf16[2048,8]{0,1:T(8,128)(2,1)} %param.17, s32[]{:T(128)S(6)} %select_n.108), kind=kOutput, calls=%fused_computation.35 | convolution fusion | flops 8394752 | bytes 4210692 | tf_op jit(solution)/shard_map/dot_general | solution.py:81
  121.5 1.0 fusion.19
  122.5 0.0 all-gather.5.cloned.1.call-update
  122.5 0.4 copy-done.1
  122.9 0.3 convert.2
  123.2 1.6 %fusion.12 = f32[4,512,2,128]{1,2,3,0:T(2,128)S(1)} fusion(f32[4,512,2,128]{1,3,2,0:T(8,128)S(1)} %bitcast.68), kind=kOutput, calls=%fused_computation.22 | output fusion | flops 66584576 | bytes 4194304 | tf_op jit(solution)/shard_map/reduce-window
  124.9 1.3 copy-done.2
  126.1 0.1 reduce-window.9
  126.2 2.4 %broadcast_add_fusion = f32[4,512,2,128]{1,2,3,0:T(2,128)S(1)} fusion(f32[4,512,2,128]{1,2,3,0:T(2,128)} %copy-done.2, f32[4,512,2]{1,2,0:T(2,128)S(1)} %slice.21), kind=kLoop, calls=%fused_computation.39 | loop fusion | flops 524288 | bytes 4210688 | tf_op jit(solution)/shard_map/reduce_window_sum
  128.6 1.7 %copy.40 = f32[4,512,2,128]{1,3,2,0:T(8,128)} copy(f32[4,512,2,128]{1,2,3,0:T(2,128)S(1)} %broadcast_add_fusion) | data formatting | bytes 4194304 | tf_op jit(solution)/shard_map/reduce_window_sum
  130.3 3.1 %fusion.14 = bf16[4,256,512]{2,1,0:T(8,128)(2,1)S(1)} fusion(f32[4,256,512]{2,1,0:T(8,128)} %bitcast.64, s32[]{:T(128)S(6)} %select_n.96, f32[256]{0:T(256)S(1)} %minimum_convert_fusion, bf16[4,256,512]{2,1,0:T(8,128)(2,1)S(1)} %bitcast.63), kind=kLoop, calls=%fused_computation.27 | loop fusion | flops 2621440 | bytes 4195332 | tf_op jit(solution)/shard_map/convert_element_type | solution.py:70
  133.4 0.0 copy-start.3
  133.4 0.0 copy-start.5
  133.4 10.9 %all-gather.5.cloned.1.call-done = bf16[1024,1024]{0,1:T(8,128)(2,1)} async-done(((bf16[1024,256]{0,1:T(8,128)(2,1)}), bf16[1024,1024]{0,1:T(8,128)(2,1)}) %all-gather.5.cloned.1.call-update) | async-done | bytes 2097168 | tf_op jit(solution)/shard_map/all_gather | solution.py:129
  144.3 2.9 %fusion.50 = f32[1024,512]{1,0:T(8,128)S(1)} fusion(bf16[1024,1024]{0,1:T(8,128)(2,1)} %all-gather.5.cloned.1.call-done, bf16[1024,512]{1,0:T(8,128)(2,1)S(1)} %copy-done), kind=kOutput, calls=%fused_computation.83 | convolution fusion | flops 1073741824 | bytes 5242880 | tf_op jit(solution)/shard_map/dot_general | solution.py:128
  147.2 0.0 copy-done.3
  147.2 0.0 copy-done.5
  147.2 1.7 %add_convert_fusion = bf16[1024,512]{1,0:T(8,128)(2,1)} fusion(f32[1024,512]{1,0:T(8,128)S(1)} %fusion.50, bf16[1024,512]{1,0:T(8,128)(2,1)S(1)} %bitcast.71, f32[512]{0:T(512)S(1)} %copy-done.5, bf16[1,512,512]{2,1,0:T(8,128)(2,1)S(1)} %copy-done.3), kind=kOutput, calls=%fused_computation.24 | convolution fusion | flops 538443776 | bytes 4720640 | tf_op jit(solution)/shard_map/dot_general | solution.py:74
  (25 shorter events, 0.1 us)
Async XLA Ops:
  6.5 137.8 %copy-start = (bf16[1024,512]{1,0:T(8,128)(2,1)S(1)}, bf16[1024,512]{1,0:T(8,128)(2,1)}, u32[]{:S(2)}) copy-start(bf16[1024,512]{1,0:T(8,128)(2,1)} %param.20) | copy-start | bytes 3145732
  8.6 31.3 %all-to-all-start = ((s32[4,1,8]{2,1,0:T(1,128)}), s32[4,1,8]{2,1,0:T(1,128)S(1)}, u32[]{:S(2)}, u32[]{:S(2)}) async-start(s32[4,1,8]{2,1,0:T(1,128)} %bitcast.9), calls=%async_computation | async-start | bytes 4096 | tf_op jit(solution)/shard_map/all_to_all | solution.py:99
  15.0 90.2 %all-gather.3.cloned.1.call-start = ((), (), s32[]{:S(2)}) async-start(), calls=%async_computation.2 | async-start | bytes 5242880 | tf_op jit(solution)/shard_map/all_gather | solution.py:79
  26.3 4.2 %copy-start.4 = (f32[2048]{0:T(1024)S(1)}, f32[2048]{0:T(1024)}, u32[]{:S(2)}) copy-start(f32[2048]{0:T(1024)} %param.21) | copy-start | bytes 24580
  30.5 4.6 %copy-start.6 = (bf16[2048,256]{1,0:T(8,128)(2,1)S(1)}, bf16[2048,256]{1,0:T(8,128)(2,1)}, u32[]{:S(2)}) copy-start(bf16[2048,256]{1,0:T(8,128)(2,1)} %param.19) | copy-start | bytes 3145732
  30.5 4.6 %copy-start.7 = (bf16[2048,256]{1,0:T(8,128)(2,1)S(1)}, bf16[2048,256]{1,0:T(8,128)(2,1)}, u32[]{:S(2)}) copy-start(bf16[2048,256]{1,0:T(8,128)(2,1)} %param.18) | copy-start | bytes 3145732
  45.1 52.4 %all-to-all-start.1 = ((bf16[4,512,512]{2,1,0:T(8,128)(2,1)}), bf16[4,512,512]{2,1,0:T(8,128)(2,1)S(1)}, u32[]{:S(2)}, u32[]{:S(2)}) async-start(bf16[4,512,512]{2,1,0:T(8,128)(2,1)} %bitcast_select_fusion.1), calls=%async_computation.1 | async-start | bytes 4194304 | tf_op jit(solution)/shard_map/all_to_all | solution.py:103
  49.6 94.7 %all-gather.5.cloned.1.call-start = ((), (), s32[]{:S(2)}) async-start(), calls=%async_computation.3 | async-start | bytes 2621440 | tf_op jit(solution)/shard_map/all_gather | solution.py:129
  121.5 1.4 copy-start.1
  124.9 1.3 copy-start.2
  133.4 13.9 %copy-start.3 = (bf16[1,512,512]{2,1,0:T(8,128)(2,1)S(1)}, bf16[1,512,512]{2,1,0:T(8,128)(2,1)}, u32[]{:S(2)}) copy-start(bf16[1,512,512]{2,1,0:T(8,128)(2,1)} %param.14) | copy-start | bytes 1572868
  133.4 13.9 %copy-start.5 = (f32[512]{0:T(512)S(1)}, f32[512]{0:T(512)}, u32[]{:S(2)}) copy-start(f32[512]{0:T(512)} %param.15) | copy-start | bytes 6148
Sparse Core Ops, SparseCore 0:
  26.5 35.3 all-gather.2
  122.6 21.6 all-gather.4
where the time goes:
time: 156 us
  waiting for transfers between devices  58.3 us (37%)
  other arithmetic  25.5 us (16%)
  matrix products  24.9 us (16%)
  local copies, waits for them, and re-layouts  16 us (10%)
  between operations  13.6 us (9%)
  starting transfers between devices  10.9 us (7%)
  blocking collectives  6.52 us (4%)
    all_to_all x1, waiting for transfers between devices, per_device(): lax.all_to_all(projected.reshape(st_count, capacity * PLEN, 2 * head_widt...  47.4 us
    all_gather x1, waiting for transfers between devices, per_device(): lax.all_gather(head_out, 'tp', axis=1, tiled=True)  10.9 us
    psum x1, blocking collectives, per_device(): square_sums = lax.psum(jnp.sum(wide_tokens * wide_tokens, axis=1), 'tp')  6.52 us
    all_to_all x1, starting transfers between devices, per_device(): lax.all_to_all(request_table, 'st', split_axis=0, concat_axis=0, tiled=True)  6.35 us
    dot_general x1, matrix products, per_device(): jnp.einsum('bhqk,bkhd->bqhd', probabilities, values, preferred_element_ty...  5.65 us
    dot_general x1, matrix products, project_rows(): jnp.dot(flat_rows, both_weights, preferred_element_type=jnp.float32)  4.79 us
    convert_element_type x1, other arithmetic, normalize_rows(): return (wide_rows * inverse * passage_gain).astype(jnp.bfloat16)  4.56 us
    all_to_all x1, starting transfers between devices, per_device(): lax.all_to_all(projected.reshape(st_count, capacity * PLEN, 2 * head_widt...  4.53 us
  transfers between devices with their start and end apart: 4, of which 2 were waited for; matrix products, arithmetic and copies ran while one was open for 26% of the time, Pallas kernels for 0%

commit v1 on v0

v1 whole, which is shorter than its diff:
```python
import functools

import jax
import jax.numpy as jnp
from jax import lax
from jax.experimental import pallas as pl
from jax.experimental.pallas import tpu as pltpu
from jax.sharding import PartitionSpec as P

HD = 128
SEQ_LEN = 256
BLK = 128
NPB = 4
MESH = pl.DeviceIdType.MESH

epsilon = 1e-06


def flip(index, mask):
    out = index
    bit = 1
    while bit <= mask:
        if mask & bit:
            out = out + bit - 2 * bit * ((index // bit) % 2)
        bit *= 2
    return out


def mixer_kernel(
    n_st,
    n_tp,
    cap,
    asked_ref,
    place_ref,
    tokens_hbm,
    norm_gain_ref,
    pool_weight_hbm,
    pool_scale_ref,
    query_weight_hbm,
    gate_weight_ref,
    key_weight_hbm,
    value_weight_hbm,
    out_weight_hbm,
    passage_gain_ref,
    store_hbm,
    out_ref,
    store,
    wk,
    wv,
    wq,
    wo,
    wp,
    tok,
    kv,
    send,
    recv,
    queries,
    gates,
    total,
    heads_all,
    load_sem,
    store_sem,
    own_sem,
    tok_far_send,
    tok_far_recv,
    tok_sib_send,
    tok_sib_recv,
    tok_fwd_send,
    tok_fwd_recv,
    kv_send,
    kv_recv,
    ho_far_send,
    ho_far_recv,
    ho_sib_send,
    ho_sib_recv,
    ho_fwd_send,
    ho_fwd_recv,
):
    st = lax.axis_index("st")
    tp = lax.axis_index("tp")
    rows = tokens_hbm.shape[0]
    width = tokens_hbm.shape[1]
    full = width * n_tp
    n_head = queries.shape[0]
    n_pass, plen = kv.shape[1], kv.shape[2]
    chunks = rows // SEQ_LEN
    fars = list(range(2, n_tp, 2))
    st_masks = list(range(n_st - 1, 0, -1))
    sib = flip(tp, 1)

    loads = [
        pltpu.make_async_copy(src, dst, load_sem.at[i])
        for i, (src, dst) in enumerate(
            [
                (key_weight_hbm, wk),
                (value_weight_hbm, wv),
                (query_weight_hbm, wq),
                (out_weight_hbm, wo),
                (pool_weight_hbm.at[0], wp),
            ]
        )
    ]
    per_step = SEQ_LEN // plen
    steps = n_pass // per_step

    def store_load(i):
        part = pl.ds(i * per_step, per_step)
        return pltpu.make_async_copy(store_hbm.at[part], store.at[part], store_sem.at[i])

    loads[0].start()
    store_load(0).start()
    loads[1].start()
    for i in range(1, steps):
        store_load(i).start()
    own_load = pltpu.make_async_copy(tokens_hbm, tok.at[tp], own_sem)
    own_load.start()
    for load in loads[2:]:
        load.start()

    barrier = pltpu.get_barrier_semaphore()
    peers = [{"tp": sib}] + [{"tp": flip(tp, m)} for m in fars]
    peers += [{"st": flip(st, m)} for m in st_masks]
    for peer in peers:
        pl.semaphore_signal(barrier, inc=1, device_id=peer, device_id_type=MESH)
    pl.semaphore_wait(barrier, len(peers))

    def remote(src, dst, send_sem, recv_sem, peer):
        return pltpu.make_async_remote_copy(
            src_ref=src,
            dst_ref=dst,
            send_sem=send_sem,
            recv_sem=recv_sem,
            device_id=peer,
            device_id_type=MESH,
        )

    def chunk_rows(r):
        return pl.ds(pl.multiple_of(r * SEQ_LEN, SEQ_LEN), SEQ_LEN)

    def tok_far(i, r):
        return remote(
            tokens_hbm.at[chunk_rows(r)],
            tok.at[tp, chunk_rows(r)],
            tok_far_send.at[i, r],
            tok_far_recv.at[i, r],
            {"tp": flip(tp, fars[i])},
        )

    def tok_sib(r):
        return remote(
            tokens_hbm.at[chunk_rows(r)],
            tok.at[tp, chunk_rows(r)],
            tok_sib_send.at[r],
            tok_sib_recv.at[r],
            {"tp": sib},
        )

    def tok_fwd(i, r):
        ref = tok.at[flip(tp, fars[i]), chunk_rows(r)]
        return remote(ref, ref, tok_fwd_send.at[i, r], tok_fwd_recv.at[i, r], {"tp": sib})

    for r in range(chunks):
        for i in range(len(fars)):
            tok_far(i, r).start()
    for r in range(chunks):
        tok_sib(r).start()

    loads[0].wait()
    loads[1].wait()

    def project(i, carry):
        store_load(i).wait()
        x = store[pl.ds(i * per_step, per_step)].reshape(SEQ_LEN, full)
        wide = x.astype(jnp.float32)
        inverse = lax.rsqrt(jnp.sum(wide * wide, axis=1, keepdims=True) / full + epsilon)
        normed = (wide * inverse * passage_gain_ref[...]).astype(jnp.bfloat16)
        k = jnp.dot(normed, wk[...], preferred_element_type=jnp.float32).astype(jnp.bfloat16)
        v = jnp.dot(normed, wv[...], preferred_element_type=jnp.float32).astype(jnp.bfloat16)
        part = pl.ds(i * per_step, per_step)
        for h in range(n_head):
            cols = slice(h * HD, (h + 1) * HD)
            kv[h, part, :, 0:HD] = k[:, cols].reshape(per_step, plen, HD)
            kv[h, part, :, HD : 2 * HD] = v[:, cols].reshape(per_step, plen, HD)
        return carry

    lax.fori_loop(0, steps, project, 0)

    def kv_copy(h, j):
        return remote(
            send.at[h, j],
            recv[h].at[pl.ds(st * cap, cap)],
            kv_send.at[h, j],
            kv_recv.at[h, j],
            {"st": flip(st, st_masks[j])},
        )

    for h in range(n_head):
        for j, mask in enumerate(st_masks):
            peer = flip(st, mask)
            for c in range(cap):
                send[h, j, c] = kv[h, asked_ref[peer, c]]
            kv_copy(h, j).start()
    for h in range(n_head):
        for c in range(cap):
            recv[h][st * cap + c] = kv[h, asked_ref[st, c]]

    own_load.wait()
    for load in loads[2:]:
        load.wait()
    window_step = tp

    def token_step(r, carry):
        for i in range(len(fars)):
            tok_far(i, r).wait_recv()
            tok_fwd(i, r).start()
        tok_sib(r).wait_recv()
        for i in range(len(fars)):
            tok_fwd(i, r).wait_recv()
        here = chunk_rows(r)
        squares = jnp.zeros((SEQ_LEN, 1), jnp.float32)
        for j in range(n_tp):
            wide = tok[j, here, :].astype(jnp.float32)
            squares = squares + jnp.sum(wide * wide, axis=1, keepdims=True)
        inverse = lax.rsqrt(squares / full + epsilon)
        query = jnp.zeros((SEQ_LEN, n_head * HD), jnp.float32)
        gate = jnp.zeros((SEQ_LEN, gate_weight_ref.shape[1]), jnp.float32)
        for j in range(n_tp):
            cols = pl.ds(j * width, width)
            wide = tok[j, here, :].astype(jnp.float32)
            normed = (wide * inverse * norm_gain_ref[:, cols]).astype(jnp.bfloat16)
            query = query + jnp.dot(normed, wq[cols, :], preferred_element_type=jnp.float32)
            gate = gate + jnp.dot(
                normed, gate_weight_ref[cols, :], preferred_element_type=jnp.float32
            )
        query = query.astype(jnp.bfloat16)
        gate = jax.nn.sigmoid(gate)
        lane = lax.broadcasted_iota(jnp.int32, gate.shape, 1)
        for h in range(n_head):
            queries[h, here, :] = query[:, h * HD : (h + 1) * HD]
            column = jnp.sum(
                jnp.where(lane == tp * n_head + h, gate, 0.0), axis=1, keepdims=True
            )
            gates[h, here, :] = jnp.broadcast_to(column, (SEQ_LEN, HD))
        own_cols = pl.ds(pl.multiple_of(tp * width, width), width)
        wide = tok[tp, here, :].astype(jnp.float32)
        mine = (wide * inverse * norm_gain_ref[:, own_cols]).astype(jnp.bfloat16)
        mine = mine.astype(jnp.float32)
        position = lax.broadcasted_iota(jnp.int32, (SEQ_LEN, width), 0)
        summed = mine
        for level in range(n_tp):
            shift = 2**level
            moved = jnp.where(position >= shift, pltpu.roll(summed, shift, axis=0), 0.0)
            summed = jnp.where(window_step >= level, summed + moved, summed)
        window = jnp.int32(2)
        for level in range(1, n_tp):
            window = jnp.where(window_step >= level, jnp.int32(2 ** (level + 1)), window)
        divisor = jnp.minimum(position + 1, window).astype(jnp.float32)
        pooled = (summed / divisor - mine).astype(jnp.bfloat16)
        mixing = jnp.dot(pooled, wp[...], preferred_element_type=jnp.float32)
        total[here, :] = mixing * pool_scale_ref[...]
        return carry

    lax.fori_loop(0, chunks, token_step, 0)

    def ho_far(h, i, r):
        ref = heads_all.at[h, tp, chunk_rows(r)]
        return remote(
            ref,
            ref,
            ho_far_send.at[h, i, r],
            ho_far_recv.at[h, i, r],
            {"tp": flip(tp, fars[i])},
        )

    def ho_sib(h, r):
        ref = heads_all.at[h, tp, chunk_rows(r)]
        return remote(ref, ref, ho_sib_send.at[h, r], ho_sib_recv.at[h, r], {"tp": sib})

    def ho_fwd(h, i, r):
        ref = heads_all.at[h, flip(tp, fars[i]), chunk_rows(r)]
        return remote(
            ref, ref, ho_fwd_send.at[h, i, r], ho_fwd_recv.at[h, i, r], {"tp": sib}
        )

    blocks = SEQ_LEN // BLK
    scale = HD ** (-0.5)

    for h in range(n_head):
        for j in range(len(st_masks)):
            kv_copy(h, j).wait_recv()

        def attend(r, carry, h=h):
            for inner in range(blocks):
                block = r * blocks + inner
                here = pl.ds(pl.multiple_of(block * BLK, BLK), BLK)
                pieces = [recv[h][place_ref[block * NPB + n]] for n in range(NPB)]
                keys = jnp.concatenate([p[:, :HD] for p in pieces], axis=0)
                vals = jnp.concatenate([p[:, HD:] for p in pieces], axis=0)
                scores = (
                    lax.dot_general(
                        queries[h, here, :],
                        keys,
                        (((1,), (1,)), ((), ())),
                        preferred_element_type=jnp.float32,
                    )
                    * scale
                )
                weights = jnp.exp(scores - jnp.max(scores, axis=1, keepdims=True))
                probs = weights / jnp.sum(weights, axis=1, keepdims=True)
                attended = jnp.dot(
                    probs.astype(jnp.bfloat16), vals, preferred_element_type=jnp.float32
                )
                heads_all[h, tp, here, :] = (attended * gates[h, here, :]).astype(jnp.bfloat16)
            for i in range(len(fars)):
                ho_far(h, i, r).start()
            ho_sib(h, r).start()
            return carry

        lax.fori_loop(0, chunks, attend, 0)

        def forward(r, carry, h=h):
            for i in range(len(fars)):
                ho_far(h, i, r).wait_recv()
                ho_fwd(h, i, r).start()
            return carry

        def finish(r, carry, h=h):
            ho_sib(h, r).wait_recv()
            for i in range(len(fars)):
                ho_fwd(h, i, r).wait_recv()
            here = chunk_rows(r)
            acc = total[here, :]
            for j in range(n_tp):
                acc = acc + jnp.dot(
                    heads_all[h, j, here, :],
                    wo[pl.ds((j * n_head + h) * HD, HD), :],
                    preferred_element_type=jnp.float32,
                )
            if h == n_head - 1:
                out_ref[here, :] = acc.astype(out_ref.dtype)
            else:
                total[here, :] = acc
            return carry

        lax.fori_loop(0, chunks, forward, 0)
        lax.fori_loop(0, chunks, finish, 0)

    def drain(r, carry):
        for i in range(len(fars)):
            tok_far(i, r).wait_send()
            tok_fwd(i, r).wait_send()
        tok_sib(r).wait_send()
        for h in range(n_head):
            for i in range(len(fars)):
                ho_far(h, i, r).wait_send()
                ho_fwd(h, i, r).wait_send()
            ho_sib(h, r).wait_send()
        return carry

    lax.fori_loop(0, chunks, drain, 0)
    for h in range(n_head):
        for j in range(len(st_masks)):
            kv_copy(h, j).wait_send()


def per_device(
    tokens,
    norm_gain,
    pool_weight,
    pool_scale,
    query_weight,
    gate_weight,
    key_weight,
    value_weight,
    out_weight,
    passage_gain,
    passage_store,
    passage_ids,
):
    n_st = lax.axis_size("st")
    n_tp = lax.axis_size("tp")
    rows, width = tokens.shape
    full = width * n_tp
    n_head = query_weight.shape[1] // HD
    n_pass, plen = passage_store.shape[:2]
    chunks = rows // SEQ_LEN
    nf = max(1, (n_tp - 1) // 2)

    flat_ids = passage_ids.reshape(-1)
    asked_count = flat_ids.shape[0]
    cap = max(2, (asked_count + n_st - 1) // n_st)
    owners = flat_ids // n_pass
    local_index = flat_ids % n_pass
    order_index = jnp.arange(asked_count, dtype=jnp.int32)
    earlier = (owners[None, :] == owners[:, None]) & (order_index[None, :] < order_index[:, None])
    slot_index = jnp.sum(earlier.astype(jnp.int32), axis=1)
    place = owners * cap + slot_index
    slot_range = jnp.arange(n_st * cap, dtype=jnp.int32)
    table = jnp.sum(
        jnp.where(place[None, :] == slot_range[:, None], local_index[None, :], 0), axis=1
    ).reshape(n_st, cap)
    asked = lax.all_to_all(table, "st", split_axis=0, concat_axis=0, tiled=True)

    any_spec = pl.BlockSpec(memory_space=pl.ANY)
    vmem = pl.BlockSpec(memory_space=pltpu.VMEM)
    smem = pl.BlockSpec(memory_space=pltpu.SMEM)
    bf = jnp.bfloat16
    dma = pltpu.SemaphoreType.DMA
    return pl.pallas_call(
        functools.partial(mixer_kernel, n_st, n_tp, cap),
        out_shape=jax.ShapeDtypeStruct((rows, width), bf),
        in_specs=[
            smem,
            smem,
            any_spec,
            vmem,
            any_spec,
            vmem,
            any_spec,
            vmem,
            any_spec,
            any_spec,
            any_spec,
            vmem,
            any_spec,
        ],
        out_specs=vmem,
        scratch_shapes=[
            pltpu.VMEM(passage_store.shape, bf),
            pltpu.VMEM(key_weight.shape, bf),
            pltpu.VMEM(value_weight.shape, bf),
            pltpu.VMEM(query_weight.shape, bf),
            pltpu.VMEM(out_weight.shape, bf),
            pltpu.VMEM(pool_weight.shape[1:], bf),
            pltpu.VMEM((n_tp, rows, width), bf),
            pltpu.VMEM((n_head, n_pass, plen, 2 * HD), bf),
            pltpu.VMEM((n_head, n_st - 1, cap, plen, 2 * HD), bf),
            [pltpu.VMEM((n_st * cap, plen, 2 * HD), bf) for _ in range(n_head)],
            pltpu.VMEM((n_head, rows, HD), bf),
            pltpu.VMEM((n_head, rows, HD), jnp.float32),
            pltpu.VMEM((rows, width), jnp.float32),
            pltpu.VMEM((n_head, n_tp, rows, HD), bf),
            dma((5,)),
            dma((n_pass * plen // SEQ_LEN,)),
            dma,
            dma((nf, chunks)),
            dma((nf, chunks)),
            dma((chunks,)),
            dma((chunks,)),
            dma((nf, chunks)),
            dma((nf, chunks)),
            dma((n_head, n_st - 1)),
            dma((n_head, n_st - 1)),
            dma((n_head, nf, chunks)),
            dma((n_head, nf, chunks)),
            dma((n_head, chunks)),
            dma((n_head, chunks)),
            dma((n_head, nf, chunks)),
            dma((n_head, nf, chunks)),
        ],
        compiler_params=pltpu.CompilerParams(
            collective_id=0, has_side_effects=True, vmem_limit_bytes=60 * 1024 * 1024
        ),
        name="mixer",
    )(
        asked,
        place,
        tokens,
        norm_gain.reshape(1, full),
        pool_weight,
        pool_scale.reshape(1, width),
        query_weight,
        gate_weight,
        key_weight,
        value_weight,
        out_weight,
        passage_gain.reshape(1, full),
        passage_store,
    )


def solution(mesh):
    in_specs = (
        P(("grp", "st"), "tp"),
        P(),
        P("tp", None, None),
        P("tp"),
        P(None, "tp"),
        P(),
        P(None, "tp"),
        P(None, "tp"),
        P(None, "tp"),
        P(),
        P(("grp", "st"), None, None),
        P(("grp", "st"), None),
    )
    out_specs = P(("grp", "st"), "tp")
    return jax.shard_map(
        per_device, mesh=mesh, in_specs=in_specs, out_specs=out_specs, check_vma=False
    )
```

time: 156 us -> 83.3 us (0.53)
  Pallas kernels: 0 us -> 65.3 us
  waiting for transfers between devices: 58.3 us -> 3.81 us
  matrix products: 24.9 us -> 0 us
  other arithmetic: 25.5 us -> 1.68 us
  between operations: 13.6 us -> 0.04 us
  local copies, waits for them, and re-layouts: 16 us -> 5.8 us
  blocking collectives: 6.52 us -> 0 us
  starting transfers between devices: 10.9 us -> 6.35 us
    pallas_call x0 -> x1, Pallas kernels: none -> 65.3 us  [per_device(): pl.pallas_call(functools.partial(mixer_kernel, n_st, n_tp, cap), out_shap...]
    all_to_all x2 -> x1, waiting for transfers between devices: 47.4 us -> 3.81 us  [per_device(): asked = lax.all_to_all(table, 'st', split_axis=0, concat_axis=0, tiled=True)]
    dot_general x7 -> x0, matrix products: 23.9 us -> none  [the longest x1 5.65 us: per_device(): jnp.einsum('bhqk,bkhd->bqhd', probabilities, values, preferred_element_ty...]
    convert_element_type x5 -> x0, other arithmetic: 11.1 us -> none  [the longest x1 4.56 us: normalize_rows(): return (wide_rows * inverse * passage_gain).astype(jnp.bfloat16)]
    all_gather x2 -> x0, waiting for transfers between devices: 11 us -> none  [the longest x1 10.9 us: per_device(): lax.all_gather(head_out, 'tp', axis=1, tiled=True)]
    psum x1 -> x0, blocking collectives: 6.52 us -> none  [per_device(): square_sums = lax.psum(jnp.sum(wide_tokens * wide_tokens, axis=1), 'tp')]
    reduce_sum x3 -> x1, other arithmetic: 5.69 us -> 0.11 us  [per_device(): jnp.sum(jnp.where(place[None, :] == slot_range[:, None], local_index[None...]
    all_to_all x2 -> x1, starting transfers between devices: 10.9 us -> 6.35 us  [per_device(): asked = lax.all_to_all(table, 'st', split_axis=0, concat_axis=0, tiled=True)]
  transfers between devices with their start and end apart: 4 -> 1, of which waited for: 2 -> 1; matrix products, arithmetic and copies ran while one was open for 26% -> 2% of each run, Pallas kernels for 0% -> 0%
where the time goes in v1:
time: 83.3 us; the launch traced here: 83 us
  Pallas kernels  65.3 us (78%)
  starting transfers between devices  6.35 us (8%)
  local copies, waits for them, and re-layouts  5.8 us (7%)
  waiting for transfers between devices  3.81 us (5%)
  other arithmetic  1.68 us (2%)
    pallas_call x1, Pallas kernels, per_device(): pl.pallas_call(functools.partial(mixer_kernel, n_st, n_tp, cap), out_shap...  65.3 us
    all_to_all x1, starting transfers between devices, per_device(): asked = lax.all_to_all(table, 'st', split_axis=0, concat_axis=0, tiled=True)  6.35 us
    unnamed x6, local copies, waits for them, and re-layouts  4.61 us
    all_to_all x1, waiting for transfers between devices, per_device(): asked = lax.all_to_all(table, 'st', split_axis=0, concat_axis=0, tiled=True)  3.81 us
  transfers between devices with their start and end apart: 1, of which 1 were waited for; matrix products, arithmetic and copies ran while one was open for 2% of the time, Pallas kernels for 0%

profile of v1, /device:TPU:0, one launch (start us, length us, event | category | flops | bytes accessed | tf_op | source)
XLA Modules:
  0.0 83.0 jit_solution(9365780340006376264)
XLA Ops:
  0.0 0.7 sign_compare_fusion
  0.7 0.7 broadcast_divide_fusion
  1.4 0.1 copy.26
  1.5 0.1 ne.56
  1.6 0.1 copy.28
  1.6 0.1 div.21
  1.7 0.1 copy.27
  1.8 0.1 rem.33
  1.9 0.2 convert_reduce_fusion
  2.1 0.0 copy-start.1
  2.1 0.1 select_reduce_fusion
  2.2 0.7 all_to_all.7
  2.9 6.3 %all-to-all-start = ((s32[4,1,8]{2,1,0:T(1,128)}), s32[4,1,8]{2,1,0:T(1,128)S(1)}, u32[]{:S(2)}, u32[]{:S(2)}) async-start(s32[4,1,8]{2,1,0:T(1,128)} %bitcast), calls=%async_computation | async-start | bytes 4096 | tf_op jit(solution)/shard_map/all_to_all | solution.py:402
  9.2 1.8 %copy.30.gate_weight_ref = bf16[2048,8]{1,0:T(8,128)(2,1)} copy(bf16[2048,8]{0,1:T(8,128)(2,1)} %param.17) | data formatting | bytes 65536 | tf_op args[5]
  11.0 3.8 %all-to-all-done = s32[4,1,8]{2,1,0:T(1,128)S(1)} async-done(((s32[4,1,8]{2,1,0:T(1,128)}), s32[4,1,8]{2,1,0:T(1,128)S(1)}, u32[]{:S(2)}, u32[]{:S(2)}) %all-to-all-start) | async-done | bytes 160 | tf_op jit(solution)/shard_map/all_to_all | solution.py:402
  14.8 0.0 copy-start
  14.8 0.0 copy-done.1
  14.8 0.6 copy-done
  15.4 65.3 %mixer.1 = bf16[1024,512]{1,0:T(8,128)(2,1)} custom-call(s32[4,8]{1,0:T(4,128)} %bitcast.7, s32[32]{0:T(128)} %copy-done.1, bf16[1024,512]{1,0:T(8,128)(2,1)} %tokens_hbm.1, f32[1,2048]{1,0:T(1,128)} %bitcast.5, bf16[1,512,512]{2,1,0:T(8,128)(2,1)} %pool_weight_hbm.1, f32[1,512]{1,0:T(1,128)} %bitcast.8, bf16[2048,256]{1,0:T(8,128)(2,1)} %query_weight_hbm.1, ...), custom_call_target="tpu_custom_call" | custom-call | tf_op jit(solution)/shard_map/mixer/pallas_call | solution.py:409
  80.7 2.3 %copy.32 = bf16[1024,512]{1,0:T(8,128)(2,1)} copy(bf16[1024,512]{1,0:T(8,128)(2,1)} %mixer.1) | data formatting | bytes 2097152
  (2 shorter events, 0.0 us)
Async XLA Ops:
  2.1 12.7 %copy-start.1 = (s32[32]{0:T(128)}, s32[32]{0:T(128)S(1)}, u32[]{:S(2)}) copy-start(s32[32]{0:T(128)S(1)} %multiply_add_fusion.place_ref) | copy-start | bytes 388
  2.9 11.9 %all-to-all-start = ((s32[4,1,8]{2,1,0:T(1,128)}), s32[4,1,8]{2,1,0:T(1,128)S(1)}, u32[]{:S(2)}, u32[]{:S(2)}) async-start(s32[4,1,8]{2,1,0:T(1,128)} %bitcast), calls=%async_computation | async-start | bytes 4096 | tf_op jit(solution)/shard_map/all_to_all | solution.py:402
  14.8 0.6 copy-start

commit v2 on v1

--- a/solution.py
+++ b/solution.py
@@ -11,6 +11,7 @@
 SEQ_LEN = 256
 BLK = 128
 NPB = 4
+LANES = 128
 MESH = pl.DeviceIdType.MESH
 
 epsilon = 1e-06
@@ -30,7 +31,7 @@
     n_st,
     n_tp,
     cap,
-    asked_ref,
+    table_ref,
     place_ref,
     tokens_hbm,
     norm_gain_ref,
@@ -44,9 +45,10 @@
     passage_gain_ref,
     store_hbm,
     out_ref,
+    asked_in,
+    asked,
     store,
-    wk,
-    wv,
+    wkv,
     wq,
     wo,
     wp,
@@ -58,6 +60,10 @@
     gates,
     total,
     heads_all,
+    ask_send,
+    ask_recv,
+    ask_load,
+    kv_load,
     load_sem,
     store_sem,
     own_sem,
@@ -92,8 +98,6 @@
         pltpu.make_async_copy(src, dst, load_sem.at[i])
         for i, (src, dst) in enumerate(
             [
-                (key_weight_hbm, wk),
-                (value_weight_hbm, wv),
                 (query_weight_hbm, wq),
                 (out_weight_hbm, wo),
                 (pool_weight_hbm.at[0], wp),
@@ -107,14 +111,25 @@
         part = pl.ds(i * per_step, per_step)
         return pltpu.make_async_copy(store_hbm.at[part], store.at[part], store_sem.at[i])
 
-    loads[0].start()
+    def kv_weight_load(h, side):
+        source = (key_weight_hbm, value_weight_hbm)[side]
+        return pltpu.make_async_copy(
+            source.at[:, pl.ds(h * HD, HD)],
+            wkv.at[h, :, pl.ds(side * HD, HD)],
+            kv_load.at[h, side],
+        )
+
     store_load(0).start()
-    loads[1].start()
+    for side in range(2):
+        kv_weight_load(0, side).start()
     for i in range(1, steps):
         store_load(i).start()
+    for h in range(1, n_head):
+        for side in range(2):
+            kv_weight_load(h, side).start()
     own_load = pltpu.make_async_copy(tokens_hbm, tok.at[tp], own_sem)
     own_load.start()
-    for load in loads[2:]:
+    for load in loads:
         load.start()
 
     barrier = pltpu.get_barrier_semaphore()
@@ -134,6 +149,15 @@
             device_id_type=MESH,
         )
 
+    def ask(j):
+        peer = flip(st, st_masks[j])
+        return remote(
+            table_ref.at[peer], asked_in.at[st], ask_send.at[j], ask_recv.at[j], {"st": peer}
+        )
+
+    for j in range(len(st_masks)):
+        ask(j).start()
+
     def chunk_rows(r):
         return pl.ds(pl.multiple_of(r * SEQ_LEN, SEQ_LEN), SEQ_LEN)
 
@@ -165,25 +189,25 @@
     for r in range(chunks):
         tok_sib(r).start()
 
-    loads[0].wait()
-    loads[1].wait()
-
-    def project(i, carry):
-        store_load(i).wait()
-        x = store[pl.ds(i * per_step, per_step)].reshape(SEQ_LEN, full)
-        wide = x.astype(jnp.float32)
-        inverse = lax.rsqrt(jnp.sum(wide * wide, axis=1, keepdims=True) / full + epsilon)
-        normed = (wide * inverse * passage_gain_ref[...]).astype(jnp.bfloat16)
-        k = jnp.dot(normed, wk[...], preferred_element_type=jnp.float32).astype(jnp.bfloat16)
-        v = jnp.dot(normed, wv[...], preferred_element_type=jnp.float32).astype(jnp.bfloat16)
-        part = pl.ds(i * per_step, per_step)
-        for h in range(n_head):
-            cols = slice(h * HD, (h + 1) * HD)
-            kv[h, part, :, 0:HD] = k[:, cols].reshape(per_step, plen, HD)
-            kv[h, part, :, HD : 2 * HD] = v[:, cols].reshape(per_step, plen, HD)
-        return carry
-
-    lax.fori_loop(0, steps, project, 0)
+    def project(h):
+        def step(i, carry):
+            part = pl.ds(i * per_step, per_step)
+            if h == 0:
+                store_load(i).wait()
+                x = store[part].reshape(SEQ_LEN, full)
+                wide = x.astype(jnp.float32)
+                inverse = lax.rsqrt(jnp.sum(wide * wide, axis=1, keepdims=True) / full + epsilon)
+                normed = (wide * inverse * passage_gain_ref[...]).astype(jnp.bfloat16)
+                store[part] = normed.reshape(per_step, plen, full)
+            else:
+                normed = store[part].reshape(SEQ_LEN, full)
+            both = jnp.dot(normed, wkv[h], preferred_element_type=jnp.float32)
+            kv[h, part] = both.astype(jnp.bfloat16).reshape(per_step, plen, 2 * HD)
+            return carry
+
+        for side in range(2):
+            kv_weight_load(h, side).wait()
+        lax.fori_loop(0, steps, step, 0)
 
     def kv_copy(h, j):
         return remote(
@@ -194,18 +218,32 @@
             {"st": flip(st, st_masks[j])},
         )
 
+    def asked_load(j):
+        if j == len(st_masks):
+            return pltpu.make_async_copy(table_ref.at[st], asked.at[st], ask_load.at[j])
+        peer = flip(st, st_masks[j])
+        return pltpu.make_async_copy(asked_in.at[peer], asked.at[peer], ask_load.at[j])
+
     for h in range(n_head):
+        project(h)
+        if h == 0:
+            for j in range(len(st_masks)):
+                ask(j).wait_recv()
+                asked_load(j).start()
+            asked_load(len(st_masks)).start()
+            for j in range(len(st_masks) + 1):
+                asked_load(j).wait()
         for j, mask in enumerate(st_masks):
             peer = flip(st, mask)
             for c in range(cap):
-                send[h, j, c] = kv[h, asked_ref[peer, c]]
+                send[h, j, c] = kv[h, asked[peer, 0, c]]
             kv_copy(h, j).start()
     for h in range(n_head):
         for c in range(cap):
-            recv[h][st * cap + c] = kv[h, asked_ref[st, c]]
+            recv[h][st * cap + c] = kv[h, asked[st, 0, c]]
 
     own_load.wait()
-    for load in loads[2:]:
+    for load in loads:
         load.wait()
     window_step = tp
 
@@ -223,14 +261,17 @@
             squares = squares + jnp.sum(wide * wide, axis=1, keepdims=True)
         inverse = lax.rsqrt(squares / full + epsilon)
         query = jnp.zeros((SEQ_LEN, n_head * HD), jnp.float32)
-        gate = jnp.zeros((SEQ_LEN, gate_weight_ref.shape[1]), jnp.float32)
+        gate = jnp.zeros((SEQ_LEN, gate_weight_ref.shape[0]), jnp.float32)
         for j in range(n_tp):
             cols = pl.ds(j * width, width)
             wide = tok[j, here, :].astype(jnp.float32)
             normed = (wide * inverse * norm_gain_ref[:, cols]).astype(jnp.bfloat16)
             query = query + jnp.dot(normed, wq[cols, :], preferred_element_type=jnp.float32)
-            gate = gate + jnp.dot(
-                normed, gate_weight_ref[cols, :], preferred_element_type=jnp.float32
+            gate = gate + lax.dot_general(
+                normed,
+                gate_weight_ref[:, cols],
+                (((1,), (1,)), ((), ())),
+                preferred_element_type=jnp.float32,
             )
         query = query.astype(jnp.bfloat16)
         gate = jax.nn.sigmoid(gate)
@@ -358,6 +399,8 @@
         return carry
 
     lax.fori_loop(0, chunks, drain, 0)
+    for j in range(len(st_masks)):
+        ask(j).wait_send()
     for h in range(n_head):
         for j in range(len(st_masks)):
             kv_copy(h, j).wait_send()
@@ -389,17 +432,18 @@
     flat_ids = passage_ids.reshape(-1)
     asked_count = flat_ids.shape[0]
     cap = max(2, (asked_count + n_st - 1) // n_st)
-    owners = flat_ids // n_pass
-    local_index = flat_ids % n_pass
+    owners = lax.div(flat_ids, jnp.int32(n_pass))
+    local_index = lax.rem(flat_ids, jnp.int32(n_pass))
     order_index = jnp.arange(asked_count, dtype=jnp.int32)
     earlier = (owners[None, :] == owners[:, None]) & (order_index[None, :] < order_index[:, None])
     slot_index = jnp.sum(earlier.astype(jnp.int32), axis=1)
     place = owners * cap + slot_index
-    slot_range = jnp.arange(n_st * cap, dtype=jnp.int32)
-    table = jnp.sum(
-        jnp.where(place[None, :] == slot_range[:, None], local_index[None, :], 0), axis=1
-    ).reshape(n_st, cap)
-    asked = lax.all_to_all(table, "st", split_axis=0, concat_axis=0, tiled=True)
+    lanes = jnp.arange(LANES, dtype=jnp.int32)
+    owner_range = jnp.arange(n_st, dtype=jnp.int32)
+    hit = (owners[None, None, None, :] == owner_range[:, None, None, None]) & (
+        slot_index[None, None, None, :] == lanes[None, None, :, None]
+    )
+    table = jnp.sum(jnp.where(hit, local_index[None, None, None, :], 0), axis=3)
 
     any_spec = pl.BlockSpec(memory_space=pl.ANY)
     vmem = pl.BlockSpec(memory_space=pltpu.VMEM)
@@ -410,7 +454,7 @@
         functools.partial(mixer_kernel, n_st, n_tp, cap),
         out_shape=jax.ShapeDtypeStruct((rows, width), bf),
         in_specs=[
-            smem,
+            vmem,
             smem,
             any_spec,
             vmem,
@@ -426,9 +470,10 @@
         ],
         out_specs=vmem,
         scratch_shapes=[
+            pltpu.VMEM((n_st, 1, LANES), jnp.int32),
+            pltpu.SMEM((n_st, 1, LANES), jnp.int32),
             pltpu.VMEM(passage_store.shape, bf),
-            pltpu.VMEM(key_weight.shape, bf),
-            pltpu.VMEM(value_weight.shape, bf),
+            pltpu.VMEM((n_head, full, 2 * HD), bf),
             pltpu.VMEM(query_weight.shape, bf),
             pltpu.VMEM(out_weight.shape, bf),
             pltpu.VMEM(pool_weight.shape[1:], bf),
@@ -440,7 +485,11 @@
             pltpu.VMEM((n_head, rows, HD), jnp.float32),
             pltpu.VMEM((rows, width), jnp.float32),
             pltpu.VMEM((n_head, n_tp, rows, HD), bf),
-            dma((5,)),
+            dma((n_st - 1,)),
+            dma((n_st - 1,)),
+            dma((n_st,)),
+            dma((n_head, 2)),
+            dma((3,)),
             dma((n_pass * plen // SEQ_LEN,)),
             dma,
             dma((nf, chunks)),
@@ -463,14 +512,14 @@
         ),
         name="mixer",
     )(
-        asked,
+        table,
         place,
         tokens,
         norm_gain.reshape(1, full),
         pool_weight,
         pool_scale.reshape(1, width),
         query_weight,
-        gate_weight,
+        gate_weight.T,
         key_weight,
         value_weight,
         out_weight,

time: 83.3 us -> 74.3 us (0.89)
  starting transfers between devices: 6.35 us -> 0 us
  Pallas kernels: 65.3 us -> 69.3 us
  waiting for transfers between devices: 3.81 us -> 0 us
  local copies, waits for them, and re-layouts: 5.8 us -> 2.59 us
    all_to_all x1 -> x0, starting transfers between devices: 6.35 us -> none  [per_device(): asked = lax.all_to_all(table, 'st', split_axis=0, concat_axis=0, tiled=True)]
    pallas_call x1, Pallas kernels: 65.3 us -> 69.3 us  [per_device(): pl.pallas_call(functools.partial(mixer_kernel, n_st, n_tp, cap), out_shap...]
    all_to_all x1 -> x0, waiting for transfers between devices: 3.81 us -> none  [per_device(): asked = lax.all_to_all(table, 'st', split_axis=0, concat_axis=0, tiled=True)]
    unnamed x6 -> x1, local copies, waits for them, and re-layouts: 4.61 us -> 2.26 us
  transfers between devices with their start and end apart: 1 -> 0, of which waited for: 1 -> 0; matrix products, arithmetic and copies ran while one was open for 2% -> 0% of each run, Pallas kernels for 0% -> 0%
where the time goes in v2:
time: 74.3 us; the launch traced here: 74.1 us
  Pallas kernels  69.3 us (93%)
  local copies, waits for them, and re-layouts  2.59 us (3%)
  other arithmetic  2.24 us (3%)
    pallas_call x1, Pallas kernels, per_device(): pl.pallas_call(functools.partial(mixer_kernel, n_st, n_tp, cap), out_shap...  69.3 us
    unnamed x1, local copies, waits for them, and re-layouts  2.26 us

profile of v2, /device:TPU:0, one launch (start us, length us, event | category | flops | bytes accessed | tf_op | source)
XLA Modules:
  0.0 74.1 jit_solution(6982266176283803832)
XLA Ops:
  0.0 0.7 broadcast_divide_fusion
  0.7 0.1 copy.17
  0.8 0.1 div.19
  0.9 0.2 convert_reduce_fusion
  1.0 0.6 multiply_add_fusion.place_ref
  1.6 0.1 iota_compare_fusion
  1.7 0.1 copy.18
  1.8 0.1 rem.11
  1.9 0.7 select_reduce_fusion
  2.6 69.3 %mixer.1 = bf16[1024,512]{1,0:T(8,128)(2,1)} custom-call(s32[4,1,128]{2,1,0:T(1,128)} %bitcast.8, s32[32]{0:T(128)} %multiply_add_fusion.place_ref, bf16[1024,512]{1,0:T(8,128)(2,1)} %tokens_hbm.1, f32[1,2048]{1,0:T(1,128)} %bitcast.6, bf16[1,512,512]{2,1,0:T(8,128)(2,1)} %pool_weight_hbm.1, f32[1,512]{1,0:T(1,128)} %bitcast.9, ...), custom_call_target="tpu_custom_call" | custom-call | tf_op jit(solution)/shard_map/mixer/pallas_call | solution.py:453
  71.8 2.3 %copy.20 = bf16[1024,512]{1,0:T(8,128)(2,1)} copy(bf16[1024,512]{1,0:T(8,128)(2,1)} %mixer.1) | data formatting | bytes 2097152
  (1 shorter events, 0.0 us)
